TPU v7x, 32 devices: a whole 2x2x4 slice. The times are simulated.
32 devices in a mesh: ep: 8 (over z, core), tp: 4 (over y, x).
Axes of the slice: x: 2, y: 2, z: 4, core: 2. Of those that a mesh axis runs over, the one named last changes fastest.
Arguments:
- tokens: bfloat16 [1024, 2048], P('ep', 'tp'), may hold values from -540 to 540
- expert_ids: int32 [1024, 2], P('ep'), may hold values from 0 to 7, all different within a row; in each aligned block of 128 rows (0 to 127, 128 to 255, ...) at most 64 rows name the same one
- gate_weights: float32 [1024, 2], P('ep'), may hold values from 0.1 to 1
- gain_in: float32 [2048], P('tp'), may hold values from 0.1 to 1.9
- gain_out: float32 [2048], P('tp'), may hold values from 0.1 to 1.9
- w_gate: bfloat16 [8, 2048, 8192], P('ep', None, 'tp'), may hold values from -0.125 to 0.125
- w_up: bfloat16 [8, 2048, 8192], P('ep', None, 'tp'), may hold values from -0.125 to 0.125
- w_down: bfloat16 [8, 8192, 2048], P('ep', 'tp'), may hold values from -0.397747564 to 0.397747564
Outputs:
- mixed: bfloat16 [1024, 2048], P('ep', 'tp')
Inputs may be any that keep to these rules, and one draw needn't show every extreme that they name: `expert_ids`: each row names 2 different experts. In the rows of one index of ep (aligned blocks of 128 rows) no expert is named by more than 64 rows, a bound that some block reaches.
All inputs are finite; a program needn't handle non-finite values.
Results may differ from a plain program's by a relative error of at most 0.018.
Values may be sent and summed in bfloat16 or wider, within the bound.
A program may use at most 64 MiB of HBM per device.

v0:
```python
import jax
import jax.numpy as jnp
from jax import lax
from jax.sharding import PartitionSpec as P

TOP = 2
NORM_EPS = 1e-06


def on_device(tokens, expert_ids, gate_weights, gain_in, gain_out, w_gate, w_up, w_down):
    count_tp = lax.axis_size("tp")
    count_ep = lax.axis_size("ep")
    tok_rows = tokens.shape[0]
    model_width = tokens.shape[1] * count_tp
    capacity = 2 * TOP * tok_rows // count_ep
    values = tokens.astype(jnp.float32)
    squares = lax.psum(jnp.sum(values * values, axis=1), "tp")
    normed = (values * lax.rsqrt(squares[:, None] / model_width + NORM_EPS) * gain_in).astype(
        jnp.bfloat16
    )
    flat_ids = expert_ids.reshape(-1)
    one_hot = (flat_ids[:, None] == jnp.arange(count_ep, dtype=jnp.int32)[None, :]).astype(
        jnp.int32
    )
    earlier = jnp.cumsum(one_hot, axis=0) - 1
    slot_index = jnp.sum(one_hot * earlier, axis=1)
    places = (flat_ids * capacity + slot_index).reshape(tok_rows, TOP)
    slot_rows = jnp.arange(count_ep * capacity, dtype=jnp.int32)
    picker = jnp.sum((slot_rows[:, None, None] == places[None, :, :]).astype(jnp.bfloat16), axis=2)
    gate_w = w_gate[0]
    up_w = w_up[0]
    down_w = w_down[0]
    outgoing = jnp.dot(picker, normed, preferred_element_type=jnp.float32).astype(jnp.bfloat16)
    arrived = lax.all_to_all(outgoing, "ep", split_axis=0, concat_axis=0, tiled=True)
    shard_part = lax.all_gather(arrived, "tp", axis=1, tiled=True)
    gate_part = jnp.dot(shard_part, gate_w, preferred_element_type=jnp.float32)
    up_part = jnp.dot(shard_part, up_w, preferred_element_type=jnp.float32)
    hidden = (jax.nn.silu(gate_part) * up_part).astype(jnp.bfloat16)
    partial_value = lax.optimization_barrier(
        jnp.dot(hidden, down_w, preferred_element_type=jnp.float32).astype(jnp.bfloat16)
    )
    summed = lax.psum_scatter(
        partial_value.astype(jnp.float32).astype(jnp.bfloat16),
        "tp",
        scatter_dimension=1,
        tiled=True,
    ).astype(jnp.float32)
    returned = lax.all_to_all(
        summed.astype(jnp.bfloat16), "ep", split_axis=0, concat_axis=0, tiled=True
    ).astype(summed.dtype)
    combined = jnp.sum(gate_weights[:, :, None] * returned[places], axis=1)
    squares_out = lax.psum(jnp.sum(combined * combined, axis=1), "tp")
    scale = lax.rsqrt(squares_out[:, None] / model_width + NORM_EPS)
    return (combined * scale * gain_out).astype(jnp.bfloat16)


def solution(mesh):
    placed = (
        P("ep", "tp"),
        P("ep", None),
        P("ep", None),
        P("tp"),
        P("tp"),
        P("ep", None, "tp"),
        P("ep", None, "tp"),
        P("ep", "tp", None),
    )
    return jax.shard_map(
        on_device, mesh=mesh, in_specs=placed, out_specs=P("ep", "tp"), check_vma=False
    )
```

profile of v0, /device:TPU:0, one launch (start us, length us, event | category | flops | bytes accessed | tf_op | source)
XLA Modules:
  0.0 177.8 jit_solution(11088431185920672371)
XLA Ops:
  6.5 0.0 all-gather.2.cloned.1.call-start
  6.5 0.8 copy.23
  7.3 0.1 eq.43
  7.5 0.1 eq.39
  7.6 0.6 reduce-window.6
  8.2 0.2 slice_reduce_fusion
  8.5 0.1 fusion.24
  8.6 0.1 reduce_sum.51
  8.7 0.1 copy.25
  8.8 0.7 compare_select_fusion
  9.5 0.1 fusion.20
  9.5 1.0 fusion.17
  10.6 11.4 %psum.14 = f32[128]{0:T(128)S(1)} all-reduce(f32[128]{0:T(128)S(1)} %fusion.17), channel_id=1, replica_groups=mesh['ep'=8,'tp'=4] {'tp'}, use_global_device_ids=true, to_apply=%region_5.6 | all-reduce | flops 128 | bytes 1024 | tf_op jit(solution)/shard_map/psum | solution.py:17
  22.0 1.3 convolution_convert_fusion
  23.2 20.1 %all_to_all.21 = bf16[8,64,512]{2,1,0:T(8,128)(2,1)} all-to-all(bf16[8,64,512]{2,1,0:T(8,128)(2,1)S(1)} %bitcast.33), channel_id=1, replica_groups=mesh['ep'=8,'tp'=4] {'ep'}, dimensions={0} | all-to-all | bytes 1048576 | tf_op jit(solution)/shard_map/all_to_all | solution.py:34
  43.3 0.0 all-gather.2.cloned.1.call-update
  43.4 0.0 reduce-scatter.2.cloned.1.call-start
  43.4 32.2 %all-gather.2.cloned.1.call-done = bf16[512,2048]{1,0:T(8,128)(2,1)} async-done(((bf16[512,512]{1,0:T(8,128)(2,1)}), bf16[512,2048]{1,0:T(8,128)(2,1)}) %all-gather.2.cloned.1.call-update) | async-done | bytes 2097168 | tf_op jit(solution)/shard_map/all_gather | solution.py:35
  75.6 0.0 copy-start.2
  75.6 10.6 %fusion.4 = f32[512,2048]{1,0:T(8,128)} fusion(bf16[512,2048]{1,0:T(8,128)(2,1)} %all-gather.2.cloned.1.call-done, bf16[1,2048,2048]{2,1,0:T(8,128)(2,1)} %param.13), kind=kOutput, calls=%fused_computation.5 | convolution fusion | flops 4294967296 | bytes 14680064 | tf_op jit(solution)/shard_map/dot_general | solution.py:36
  86.2 0.0 copy-done.2
  86.2 0.0 copy-start.1
  86.2 17.5 %fusion.10 = bf16[512,2048]{1,0:T(8,128)(2,1)} fusion(bf16[1,2048,2048]{2,1,0:T(8,128)(2,1)} %param.15, f32[512,2048]{1,0:T(8,128)} %fusion.4, bf16[512,2048]{1,0:T(8,128)(2,1)S(1)} %copy-done.2, bf16[1,2048,2048]{2,1,0:T(8,128)(2,1)} %param.14), kind=kOutput, calls=%fused_computation.8 | convolution fusion | flops 8597274624 | bytes 25165824 | tf_op jit(solution)/shard_map/dot_general | solution.py:40
  103.7 0.0 reduce-scatter.2.cloned.1.call-update
  103.7 35.3 %reduce-scatter.2.cloned.1.call-done = bf16[512,512]{1,0:T(8,128)(2,1)} async-done(((bf16[512,2048]{1,0:T(8,128)(2,1)}), bf16[512,512]{1,0:T(8,128)(2,1)}) %reduce-scatter.2.cloned.1.call-update) | async-done | bytes 524304 | tf_op jit(solution)/shard_map/reduce_scatter | solution.py:42
  139.0 4.6 %all-to-all-start.1 = ((bf16[8,64,512]{2,1,0:T(8,128)(2,1)}), bf16[8,64,512]{2,1,0:T(8,128)(2,1)S(1)}, u32[]{:S(2)}, u32[]{:S(2)}) async-start(bf16[8,64,512]{2,1,0:T(8,128)(2,1)} %bitcast.34), calls=%async_computation.2 | async-start | bytes 1048576 | tf_op jit(solution)/shard_map/all_to_all | solution.py:48
  143.6 0.1 copy.26
  143.8 0.1 reshape.49
  143.9 0.0 copy-done.1
  143.9 0.1 copy.22
  144.0 0.0 copy-start
  144.0 14.9 %all-to-all-done.1 = bf16[8,64,512]{2,1,0:T(8,128)(2,1)S(1)} async-done(((bf16[8,64,512]{2,1,0:T(8,128)(2,1)}), bf16[8,64,512]{2,1,0:T(8,128)(2,1)S(1)}, u32[]{:S(2)}, u32[]{:S(2)}) %all-to-all-start.1) | async-done | bytes 524320 | tf_op jit(solution)/shard_map/all_to_all | solution.py:48
  159.0 0.1 bitcast_convert_fusion
  159.1 1.0 gather_fusion
  160.1 0.3 reshape.48
  160.4 0.7 multiply_reduce_fusion
  161.1 0.1 multiply_reduce_fusion.1
  161.2 8.9 %psum.15 = f32[128]{0:T(128)S(1)} all-reduce(f32[128]{0:T(128)S(1)} %multiply_reduce_fusion.1), channel_id=1, replica_groups=mesh['ep'=8,'tp'=4] {'tp'}, use_global_device_ids=true, to_apply=%region_9.10 | all-reduce | flops 128 | bytes 1024 | tf_op jit(solution)/shard_map/psum | solution.py:52
  170.2 0.0 copy-done
  170.2 0.8 multiply_convert_fusion.1
  (6 shorter events, 0.1 us)
Async XLA Ops:
  6.5 69.1 %all-gather.2.cloned.1.call-start = ((), (), s32[]{:S(2)}) async-start(), calls=%async_computation.3 | async-start | bytes 2621440 | tf_op jit(solution)/shard_map/all_gather | solution.py:35
  43.4 95.7 %reduce-scatter.2.cloned.1.call-start = ((), (), s32[]{:S(2)}) async-start(), calls=%async_computation.4 | async-start | bytes 2621440 | tf_op jit(solution)/shard_map/reduce_scatter | solution.py:42
  75.6 10.6 %copy-start.2 = (bf16[512,2048]{1,0:T(8,128)(2,1)S(1)}, bf16[512,2048]{1,0:T(8,128)(2,1)}, u32[]{:S(2)}) copy-start(bf16[512,2048]{1,0:T(8,128)(2,1)} %all-gather.2.cloned.1.call-done) | copy-start | bytes 6291460
  86.2 57.7 %copy-start.1 = (f32[128,2]{0,1:T(2,128)S(1)}, f32[128,2]{0,1:T(2,128)}, u32[]{:S(2)}) copy-start(f32[128,2]{0,1:T(2,128)} %param.10) | copy-start | bytes 3076
  139.0 19.9 %all-to-all-start.1 = ((bf16[8,64,512]{2,1,0:T(8,128)(2,1)}), bf16[8,64,512]{2,1,0:T(8,128)(2,1)S(1)}, u32[]{:S(2)}, u32[]{:S(2)}) async-start(bf16[8,64,512]{2,1,0:T(8,128)(2,1)} %bitcast.34), calls=%async_computation.2 | async-start | bytes 1048576 | tf_op jit(solution)/shard_map/all_to_all | solution.py:48
  144.0 26.2 %copy-start = (f32[512]{0:T(512)S(1)}, f32[512]{0:T(512)}, u32[]{:S(2)}) copy-start(f32[512]{0:T(512)} %param.12) | copy-start | bytes 6148
Sparse Core Ops, SparseCore 0:
  43.5 32.0 all-gather.1
  103.8 35.1 reduce-scatter.1
where the time goes:
time: 178 us
  waiting for transfers between devices  82.5 us (46%)
  blocking collectives  40.4 us (23%)
  matrix products  29.3 us (16%)
  between operations  13.5 us (8%)
  starting transfers between devices  4.65 us (3%)
  other arithmetic  4.23 us (2%)
  local copies, waits for them, and re-layouts  3.14 us (2%)
    reduce_scatter x1, waiting for transfers between devices, on_device(): lax.psum_scatter(partial_value.astype(jnp.float32).astype(jnp.bfloat16),...  35.3 us
    all_gather x1, waiting for transfers between devices, on_device(): shard_part = lax.all_gather(arrived, 'tp', axis=1, tiled=True)  32.2 us
    all_to_all x1, blocking collectives, on_device(): lax.all_to_all(outgoing, 'ep', split_axis=0, concat_axis=0, tiled=True)  20.1 us
    dot_general x1, matrix products, on_device(): jnp.dot(hidden, down_w, preferred_element_type=jnp.float32)  17.5 us
    all_to_all x1, waiting for transfers between devices, on_device(): lax.all_to_all(summed.astype(jnp.bfloat16), 'ep', split_axis=0, concat_ax...  14.9 us
    psum x1, blocking collectives, on_device(): squares = lax.psum(jnp.sum(values * values, axis=1), 'tp')  11.4 us
    dot_general x1, matrix products, on_device(): gate_part = jnp.dot(shard_part, gate_w, preferred_element_type=jnp.float32)  10.6 us
    psum x1, blocking collectives, on_device(): squares_out = lax.psum(jnp.sum(combined * combined, axis=1), 'tp')  8.94 us
  transfers between devices with their start and end apart: 3, of which 3 were waited for; matrix products, arithmetic and copies ran while one was open for 0% of the time, Pallas kernels for 0%

commit v1 on v0

--- a/solution.py
+++ b/solution.py
@@ -5,6 +5,12 @@
 
 TOP = 2
 NORM_EPS = 1e-06
+
+
+def add_all(value, axis):
+    shards = lax.all_gather(value, axis, axis=0, tiled=False)
+    total = shards.sum(axis=0)
+    return total
 
 
 def on_device(tokens, expert_ids, gate_weights, gain_in, gain_out, w_gate, w_up, w_down):
@@ -49,7 +55,7 @@
         summed.astype(jnp.bfloat16), "ep", split_axis=0, concat_axis=0, tiled=True
     ).astype(summed.dtype)
     combined = jnp.sum(gate_weights[:, :, None] * returned[places], axis=1)
-    squares_out = lax.psum(jnp.sum(combined * combined, axis=1), "tp")
+    squares_out = add_all(jnp.sum(combined * combined, axis=1), "tp")
     scale = lax.rsqrt(squares_out[:, None] / model_width + NORM_EPS)
     return (combined * scale * gain_out).astype(jnp.bfloat16)
 

time: 178 us -> 177 us (level)
    psum x1 -> x0, blocking collectives: 8.94 us -> none  [on_device(): squares_out = lax.psum(jnp.sum(combined * combined, axis=1), 'tp')]
    all_gather x0 -> x1, blocking collectives: none -> 7.91 us  [add_all(): shards = lax.all_gather(value, axis, axis=0, tiled=False)]
where the time goes in v1:
time: 177 us
  waiting for transfers between devices  82.5 us (47%)
  blocking collectives  39.4 us (22%)
  matrix products  29.3 us (17%)
  between operations  13.5 us (8%)
  starting transfers between devices  4.65 us (3%)
  other arithmetic  4.25 us (2%)
  local copies, waits for them, and re-layouts  3.14 us (2%)
    reduce_scatter x1, waiting for transfers between devices, on_device(): lax.psum_scatter(partial_value.astype(jnp.float32).astype(jnp.bfloat16),...  35.3 us
    all_gather x1, waiting for transfers between devices, on_device(): shard_part = lax.all_gather(arrived, 'tp', axis=1, tiled=True)  32.2 us
    all_to_all x1, blocking collectives, on_device(): lax.all_to_all(outgoing, 'ep', split_axis=0, concat_axis=0, tiled=True)  20.1 us
    dot_general x1, matrix products, on_device(): jnp.dot(hidden, down_w, preferred_element_type=jnp.float32)  17.5 us
    all_to_all x1, waiting for transfers between devices, on_device(): lax.all_to_all(summed.astype(jnp.bfloat16), 'ep', split_axis=0, concat_ax...  14.9 us
    psum x1, blocking collectives, on_device(): squares = lax.psum(jnp.sum(values * values, axis=1), 'tp')  11.4 us
    dot_general x1, matrix products, on_device(): gate_part = jnp.dot(shard_part, gate_w, preferred_element_type=jnp.float32)  10.6 us
    all_gather x1, blocking collectives, add_all(): shards = lax.all_gather(value, axis, axis=0, tiled=False)  7.91 us
  transfers between devices with their start and end apart: 3, of which 3 were waited for; matrix products, arithmetic and copies ran while one was open for 0% of the time, Pallas kernels for 0%

profile of v1, /device:TPU:0, one launch (start us, length us, event | category | flops | bytes accessed | tf_op | source)
XLA Modules:
  0.0 176.8 jit_solution(2650012142130354864)
XLA Ops:
  6.5 0.0 all-gather.4.cloned.1.call-start
  6.5 0.8 copy.28
  7.3 0.1 eq.43
  7.5 0.1 eq.39
  7.6 0.6 reduce-window.6
  8.2 0.2 slice_reduce_fusion
  8.5 0.1 fusion.24
  8.6 0.1 reduce_sum.60
  8.7 0.1 copy.30
  8.8 0.7 compare_select_fusion
  9.5 0.1 fusion.20
  9.5 1.0 fusion.17
  10.6 11.4 %psum.7 = f32[128]{0:T(128)S(1)} all-reduce(f32[128]{0:T(128)S(1)} %fusion.17), channel_id=1, replica_groups=mesh['ep'=8,'tp'=4] {'tp'}, use_global_device_ids=true, to_apply=%region_5.6 | all-reduce | flops 128 | bytes 1024 | tf_op jit(solution)/shard_map/psum | solution.py:23
  22.0 1.3 convolution_convert_fusion
  23.2 20.1 %all_to_all.21 = bf16[8,64,512]{2,1,0:T(8,128)(2,1)} all-to-all(bf16[8,64,512]{2,1,0:T(8,128)(2,1)S(1)} %bitcast.34), channel_id=1, replica_groups=mesh['ep'=8,'tp'=4] {'ep'}, dimensions={0} | all-to-all | bytes 1048576 | tf_op jit(solution)/shard_map/all_to_all | solution.py:40
  43.3 0.0 all-gather.4.cloned.1.call-update
  43.4 0.0 reduce-scatter.2.cloned.1.call-start
  43.4 32.2 %all-gather.4.cloned.1.call-done = bf16[512,2048]{1,0:T(8,128)(2,1)} async-done(((bf16[512,512]{1,0:T(8,128)(2,1)}), bf16[512,2048]{1,0:T(8,128)(2,1)}) %all-gather.4.cloned.1.call-update) | async-done | bytes 2097168 | tf_op jit(solution)/shard_map/all_gather | solution.py:41
  75.6 0.0 copy-start.2
  75.6 10.6 %fusion.4 = f32[512,2048]{1,0:T(8,128)} fusion(bf16[512,2048]{1,0:T(8,128)(2,1)} %all-gather.4.cloned.1.call-done, bf16[1,2048,2048]{2,1,0:T(8,128)(2,1)} %param.13), kind=kOutput, calls=%fused_computation.5 | convolution fusion | flops 4294967296 | bytes 14680064 | tf_op jit(solution)/shard_map/dot_general | solution.py:42
  86.2 0.0 copy-done.2
  86.2 0.0 copy-start.1
  86.2 17.5 %fusion.10 = bf16[512,2048]{1,0:T(8,128)(2,1)} fusion(bf16[1,2048,2048]{2,1,0:T(8,128)(2,1)} %param.15, f32[512,2048]{1,0:T(8,128)} %fusion.4, bf16[512,2048]{1,0:T(8,128)(2,1)S(1)} %copy-done.2, bf16[1,2048,2048]{2,1,0:T(8,128)(2,1)} %param.14), kind=kOutput, calls=%fused_computation.8 | convolution fusion | flops 8597274624 | bytes 25165824 | tf_op jit(solution)/shard_map/dot_general | solution.py:46
  103.7 0.0 reduce-scatter.2.cloned.1.call-update
  103.7 35.3 %reduce-scatter.2.cloned.1.call-done = bf16[512,512]{1,0:T(8,128)(2,1)} async-done(((bf16[512,2048]{1,0:T(8,128)(2,1)}), bf16[512,512]{1,0:T(8,128)(2,1)}) %reduce-scatter.2.cloned.1.call-update) | async-done | bytes 524304 | tf_op jit(solution)/shard_map/reduce_scatter | solution.py:48
  139.0 4.6 %all-to-all-start.1 = ((bf16[8,64,512]{2,1,0:T(8,128)(2,1)}), bf16[8,64,512]{2,1,0:T(8,128)(2,1)S(1)}, u32[]{:S(2)}, u32[]{:S(2)}) async-start(bf16[8,64,512]{2,1,0:T(8,128)(2,1)} %bitcast.35), calls=%async_computation.2 | async-start | bytes 1048576 | tf_op jit(solution)/shard_map/all_to_all | solution.py:54
  143.6 0.1 copy.31
  143.8 0.1 reshape.53
  143.9 0.0 copy-done.1
  143.9 0.1 copy.27
  144.0 0.0 copy-start
  144.0 14.9 %all-to-all-done.1 = bf16[8,64,512]{2,1,0:T(8,128)(2,1)S(1)} async-done(((bf16[8,64,512]{2,1,0:T(8,128)(2,1)}), bf16[8,64,512]{2,1,0:T(8,128)(2,1)S(1)}, u32[]{:S(2)}, u32[]{:S(2)}) %all-to-all-start.1) | async-done | bytes 524320 | tf_op jit(solution)/shard_map/all_to_all | solution.py:54
  159.0 0.1 bitcast_convert_fusion
  159.1 1.0 gather_fusion
  160.1 0.3 reshape.52
  160.4 0.7 multiply_reduce_fusion
  161.1 0.1 multiply_reduce_fusion.1
  161.2 7.9 %all-gather.1 = f32[4,1,128]{2,1,0:T(1,128)S(1)} all-gather(f32[1,1,128]{2,1,0:T(1,128)S(1)} %bitcast.36), channel_id=2, replica_groups=mesh['ep'=8,'tp'=4] {'tp'}, dimensions={0}, use_global_device_ids=true | all-gather | bytes 2560 | tf_op jit(solution)/shard_map/all_gather | solution.py:11
  169.2 0.0 copy-done
  169.2 0.8 multiply_convert_fusion.1
  (7 shorter events, 0.1 us)
Async XLA Ops:
  6.5 69.1 %all-gather.4.cloned.1.call-start = ((), (), s32[]{:S(2)}) async-start(), calls=%async_computation.3 | async-start | bytes 2621440 | tf_op jit(solution)/shard_map/all_gather | solution.py:41
  43.4 95.7 %reduce-scatter.2.cloned.1.call-start = ((), (), s32[]{:S(2)}) async-start(), calls=%async_computation.4 | async-start | bytes 2621440 | tf_op jit(solution)/shard_map/reduce_scatter | solution.py:48
  75.6 10.6 %copy-start.2 = (bf16[512,2048]{1,0:T(8,128)(2,1)S(1)}, bf16[512,2048]{1,0:T(8,128)(2,1)}, u32[]{:S(2)}) copy-start(bf16[512,2048]{1,0:T(8,128)(2,1)} %all-gather.4.cloned.1.call-done) | copy-start | bytes 6291460
  86.2 57.7 %copy-start.1 = (f32[128,2]{0,1:T(2,128)S(1)}, f32[128,2]{0,1:T(2,128)}, u32[]{:S(2)}) copy-start(f32[128,2]{0,1:T(2,128)} %param.10) | copy-start | bytes 3076
  139.0 19.9 %all-to-all-start.1 = ((bf16[8,64,512]{2,1,0:T(8,128)(2,1)}), bf16[8,64,512]{2,1,0:T(8,128)(2,1)S(1)}, u32[]{:S(2)}, u32[]{:S(2)}) async-start(bf16[8,64,512]{2,1,0:T(8,128)(2,1)} %bitcast.35), calls=%async_computation.2 | async-start | bytes 1048576 | tf_op jit(solution)/shard_map/all_to_all | solution.py:54
  144.0 25.1 %copy-start = (f32[512]{0:T(512)S(1)}, f32[512]{0:T(512)}, u32[]{:S(2)}) copy-start(f32[512]{0:T(512)} %param.12) | copy-start | bytes 6148
Sparse Core Ops, SparseCore 0:
  43.5 32.0 all-gather.3
  103.8 35.1 reduce-scatter.1

commit v2 on v0

--- a/solution.py
+++ b/solution.py
@@ -2,9 +2,13 @@
 import jax.numpy as jnp
 from jax import lax
 from jax.sharding import PartitionSpec as P
+from jax.lax import all_gather
 
 TOP = 2
 NORM_EPS = 1e-06
+order_quarters = lambda piece_in, axis_name: jnp.concatenate(
+    all_gather(piece_in, axis_name), axis=1
+)
 
 
 def on_device(tokens, expert_ids, gate_weights, gain_in, gain_out, w_gate, w_up, w_down):
@@ -32,7 +36,7 @@
     down_w = w_down[0]
     outgoing = jnp.dot(picker, normed, preferred_element_type=jnp.float32).astype(jnp.bfloat16)
     arrived = lax.all_to_all(outgoing, "ep", split_axis=0, concat_axis=0, tiled=True)
-    shard_part = lax.all_gather(arrived, "tp", axis=1, tiled=True)
+    shard_part = order_quarters(arrived, "tp")
     gate_part = jnp.dot(shard_part, gate_w, preferred_element_type=jnp.float32)
     up_part = jnp.dot(shard_part, up_w, preferred_element_type=jnp.float32)
     hidden = (jax.nn.silu(gate_part) * up_part).astype(jnp.bfloat16)

time: 178 us -> 181 us (1.017)
  local copies, waits for them, and re-layouts: 3.14 us -> 5.92 us
    all_gather x0 -> x1, local copies, waits for them, and re-layouts: none -> 2.79 us  [all_gather(piece_in, axis_name)]
where the time goes in v2:
time: 181 us; the launch traced here: 180 us
  waiting for transfers between devices  82.6 us (46%)
  blocking collectives  40.4 us (22%)
  matrix products  28.7 us (16%)
  between operations  13.5 us (7%)
  local copies, waits for them, and re-layouts  5.92 us (3%)
  starting transfers between devices  4.65 us (3%)
  other arithmetic  4.23 us (2%)
    reduce_scatter x1, waiting for transfers between devices, on_device(): lax.psum_scatter(partial_value.astype(jnp.float32).astype(jnp.bfloat16),...  35.3 us
    all_gather x1, waiting for transfers between devices, all_gather(piece_in, axis_name)  32.3 us
    all_to_all x1, blocking collectives, on_device(): lax.all_to_all(outgoing, 'ep', split_axis=0, concat_axis=0, tiled=True)  20.1 us
    dot_general x1, matrix products, on_device(): jnp.dot(hidden, down_w, preferred_element_type=jnp.float32)  18 us
    all_to_all x1, waiting for transfers between devices, on_device(): lax.all_to_all(summed.astype(jnp.bfloat16), 'ep', split_axis=0, concat_ax...  14.9 us
    psum x1, blocking collectives, on_device(): squares = lax.psum(jnp.sum(values * values, axis=1), 'tp')  11.4 us
    dot_general x1, matrix products, on_device(): gate_part = jnp.dot(shard_part, gate_w, preferred_element_type=jnp.float32)  9.43 us
    psum x1, blocking collectives, on_device(): squares_out = lax.psum(jnp.sum(combined * combined, axis=1), 'tp')  8.94 us
  transfers between devices with their start and end apart: 3, of which 3 were waited for; matrix products, arithmetic and copies ran while one was open for 0% of the time, Pallas kernels for 0%

profile of v2, /device:TPU:0, one launch (start us, length us, event | category | flops | bytes accessed | tf_op | source)
XLA Modules:
  0.0 180.1 jit_solution(5731504696938454310)
XLA Ops:
  6.5 0.0 all-gather.2.cloned.1.call-start
  6.5 0.8 copy.37
  7.3 0.1 eq.43
  7.5 0.1 eq.39
  7.6 0.6 reduce-window.6
  8.2 0.2 slice_reduce_fusion
  8.5 0.1 fusion.24
  8.6 0.1 reduce_sum.51
  8.7 0.1 copy.39
  8.8 0.7 compare_select_fusion
  9.5 0.1 fusion.20
  9.5 1.0 fusion.17
  10.6 11.4 %psum.14 = f32[128]{0:T(128)S(1)} all-reduce(f32[128]{0:T(128)S(1)} %fusion.17), channel_id=1, replica_groups=mesh['ep'=8,'tp'=4] {'tp'}, use_global_device_ids=true, to_apply=%region_5.6 | all-reduce | flops 128 | bytes 1024 | tf_op jit(solution)/shard_map/psum | solution.py:21
  22.0 1.3 convolution_convert_fusion
  23.2 20.1 %all_to_all.18 = bf16[8,64,512]{2,1,0:T(8,128)(2,1)} all-to-all(bf16[8,64,512]{2,1,0:T(8,128)(2,1)S(1)} %bitcast.38), channel_id=1, replica_groups=mesh['ep'=8,'tp'=4] {'ep'}, dimensions={0} | all-to-all | bytes 1048576 | tf_op jit(solution)/shard_map/all_to_all | solution.py:38
  43.3 0.0 all-gather.2.cloned.1.call-update
  43.4 0.0 reduce-scatter.2.cloned.1.call-start
  43.4 32.3 %all-gather.2.cloned.1.call-done = bf16[4,512,512]{2,1,0:T(8,128)(2,1)} async-done(((bf16[1,512,512]{2,1,0:T(8,128)(2,1)}), bf16[4,512,512]{2,1,0:T(8,128)(2,1)}) %all-gather.2.cloned.1.call-update) | async-done | bytes 2097168 | tf_op jit(solution)/shard_map/all_gather | solution.py:10
  75.8 2.8 %copy.40 = bf16[4,512,512]{1,2,0:T(8,128)(2,1)S(1)} copy(bf16[4,512,512]{2,1,0:T(8,128)(2,1)} %all-gather.2.cloned.1.call-done) | data formatting | bytes 4194304 | tf_op jit(solution)/shard_map/all_gather | solution.py:10
  78.5 9.4 %fusion.4 = f32[512,2048]{1,0:T(8,128)} fusion(bf16[512,2048]{0,1:T(8,128)(2,1)S(1)} %bitcast.35, bf16[1,2048,2048]{2,1,0:T(8,128)(2,1)} %param.13), kind=kOutput, calls=%fused_computation.5 | convolution fusion | flops 4294967296 | bytes 14680064 | tf_op jit(solution)/shard_map/dot_general | solution.py:40
  88.0 0.0 copy-start.1
  88.0 18.0 %fusion.10 = bf16[512,2048]{1,0:T(8,128)(2,1)} fusion(bf16[1,2048,2048]{2,1,0:T(8,128)(2,1)} %param.15, f32[512,2048]{1,0:T(8,128)} %fusion.4, bf16[512,2048]{0,1:T(8,128)(2,1)S(1)} %bitcast.36, bf16[1,2048,2048]{2,1,0:T(8,128)(2,1)} %param.14), kind=kOutput, calls=%fused_computation.8 | convolution fusion | flops 8597274624 | bytes 25165824 | tf_op jit(solution)/shard_map/dot_general | solution.py:44
  106.0 0.0 reduce-scatter.2.cloned.1.call-update
  106.0 35.3 %reduce-scatter.2.cloned.1.call-done = bf16[512,512]{1,0:T(8,128)(2,1)} async-done(((bf16[512,2048]{1,0:T(8,128)(2,1)}), bf16[512,512]{1,0:T(8,128)(2,1)}) %reduce-scatter.2.cloned.1.call-update) | async-done | bytes 524304 | tf_op jit(solution)/shard_map/reduce_scatter | solution.py:46
  141.4 4.6 %all-to-all-start.1 = ((bf16[8,64,512]{2,1,0:T(8,128)(2,1)}), bf16[8,64,512]{2,1,0:T(8,128)(2,1)S(1)}, u32[]{:S(2)}, u32[]{:S(2)}) async-start(bf16[8,64,512]{2,1,0:T(8,128)(2,1)} %bitcast.39), calls=%async_computation.2 | async-start | bytes 1048576 | tf_op jit(solution)/shard_map/all_to_all | solution.py:52
  146.0 0.1 copy.41
  146.1 0.1 reshape.58
  146.2 0.0 copy-done.1
  146.2 0.1 copy.36
  146.3 0.0 copy-start
  146.3 14.9 %all-to-all-done.1 = bf16[8,64,512]{2,1,0:T(8,128)(2,1)S(1)} async-done(((bf16[8,64,512]{2,1,0:T(8,128)(2,1)}), bf16[8,64,512]{2,1,0:T(8,128)(2,1)S(1)}, u32[]{:S(2)}, u32[]{:S(2)}) %all-to-all-start.1) | async-done | bytes 524320 | tf_op jit(solution)/shard_map/all_to_all | solution.py:52
  161.3 0.1 bitcast_convert_fusion
  161.4 1.0 gather_fusion
  162.4 0.3 reshape.57
  162.7 0.7 multiply_reduce_fusion
  163.4 0.1 multiply_reduce_fusion.1
  163.5 8.9 %psum.15 = f32[128]{0:T(128)S(1)} all-reduce(f32[128]{0:T(128)S(1)} %multiply_reduce_fusion.1), channel_id=1, replica_groups=mesh['ep'=8,'tp'=4] {'tp'}, use_global_device_ids=true, to_apply=%region_9.10 | all-reduce | flops 128 | bytes 1024 | tf_op jit(solution)/shard_map/psum | solution.py:56
  172.5 0.0 copy-done
  172.5 0.8 multiply_convert_fusion.1
  (6 shorter events, 0.1 us)
Async XLA Ops:
  6.5 69.2 %all-gather.2.cloned.1.call-start = ((), (), s32[]{:S(2)}) async-start(), calls=%async_computation.3 | async-start | bytes 2621440 | tf_op jit(solution)/shard_map/all_gather | solution.py:10
  43.4 98.0 %reduce-scatter.2.cloned.1.call-start = ((), (), s32[]{:S(2)}) async-start(), calls=%async_computation.4 | async-start | bytes 2621440 | tf_op jit(solution)/shard_map/reduce_scatter | solution.py:46
  88.0 58.2 %copy-start.1 = (f32[128,2]{0,1:T(2,128)S(1)}, f32[128,2]{0,1:T(2,128)}, u32[]{:S(2)}) copy-start(f32[128,2]{0,1:T(2,128)} %param.10) | copy-start | bytes 3076
  141.4 19.9 %all-to-all-start.1 = ((bf16[8,64,512]{2,1,0:T(8,128)(2,1)}), bf16[8,64,512]{2,1,0:T(8,128)(2,1)S(1)}, u32[]{:S(2)}, u32[]{:S(2)}) async-start(bf16[8,64,512]{2,1,0:T(8,128)(2,1)} %bitcast.39), calls=%async_computation.2 | async-start | bytes 1048576 | tf_op jit(solution)/shard_map/all_to_all | solution.py:52
  146.3 26.2 %copy-start = (f32[512]{0:T(512)S(1)}, f32[512]{0:T(512)}, u32[]{:S(2)}) copy-start(f32[512]{0:T(512)} %param.12) | copy-start | bytes 6148
Sparse Core Ops, SparseCore 0:
  43.5 32.2 all-gather.1
  106.1 35.1 reduce-scatter.1
